TPU v7x, 32 devices: a whole 2x2x4 slice. The times are simulated.
32 devices in a mesh: ra: 4 (over z), cb: 4 (over y, x), dp: 2 (over core).
Axes of the slice: x: 2, y: 2, z: 4, core: 2. Of those that a mesh axis runs over, the one named last changes fastest.
Arguments:
- tokens: bfloat16 [128, 4096], P('dp', 'ra'), may hold values from -45 to 45
- gain_first: bfloat16 [4096], P('ra'), may hold values from 0.099609375 to 1.8984375
- up_first: float32 [4096, 16384], P('ra', 'cb'), may hold values from -0.125 to 0.125
- up_scale_first: float32 [16384], P('cb'), may hold values from 0.5 to 2
- down_first: float32 [16384, 4096], P('cb', 'ra'), may hold values from -0.046875 to 0.046875
- down_scale_first: float32 [4096], P('ra'), may hold values from 0.5 to 2
- gain_second: bfloat16 [4096], P('ra'), may hold values from 0.099609375 to 1.8984375
- up_second: float32 [4096, 16384], P('ra', 'cb'), may hold values from -0.125 to 0.125
- up_scale_second: float32 [16384], P('cb'), may hold values from 0.5 to 2
- down_second: float32 [16384, 4096], P('cb', 'ra'), may hold values from -0.046875 to 0.046875
- down_scale_second: float32 [4096], P('ra'), may hold values from 0.5 to 2
Outputs:
- mixed_out: bfloat16 [128, 4096], P('dp', 'ra')
All inputs are finite; a program needn't handle non-finite values.
Results may differ from a plain program's by a relative error of at most 0.02.
Values may be sent and summed in bfloat16 or wider, within the bound.
A program may use at most 128 MiB of HBM per device.

v0:
```python
import jax
import jax.numpy as jnp
from jax import lax
from jax.sharding import PartitionSpec as P

epsilon = 1e-06
residual_share = 0.25


def sub_layer(inputs, norm_gain, up_weight, up_scale, down_weight, down_scale):
    values = inputs.astype(jnp.float32)
    full_width = inputs.shape[1] * lax.axis_size("ra")
    squares = lax.psum(jnp.sum(values * values, axis=1, keepdims=True), "ra")
    inverse = lax.rsqrt(squares / full_width + epsilon)
    normed = (values * inverse * norm_gain.astype(jnp.float32)).astype(jnp.bfloat16)
    partial_value = jnp.dot(
        normed, up_weight.astype(jnp.bfloat16), preferred_element_type=jnp.float32
    )
    shares = lax.psum_scatter(partial_value, "ra", scatter_dimension=1, tiled=True)
    share_width = shares.shape[1]
    own_scale = lax.dynamic_slice_in_dim(
        up_scale, lax.axis_index("ra") * share_width, share_width, 0
    )
    own_units = jnp.square(jax.nn.relu(shares * own_scale)).astype(jnp.bfloat16)
    hidden = lax.all_gather(own_units, "ra", axis=1, tiled=True)
    projected = jnp.dot(
        hidden, down_weight.astype(jnp.bfloat16), preferred_element_type=jnp.float32
    ).astype(jnp.bfloat16)
    projected = lax.optimization_barrier(projected).astype(jnp.float32)
    total = lax.psum(projected.astype(jnp.bfloat16), "cb").astype(jnp.float32)
    return (residual_share * values + total * down_scale).astype(jnp.bfloat16)


def shards(
    tokens,
    gain_first,
    up_first,
    up_scale_first,
    down_first,
    down_scale_first,
    gain_second,
    up_second,
    up_scale_second,
    down_second,
    down_scale_second,
):
    carried = sub_layer(tokens, gain_first, up_first, up_scale_first, down_first, down_scale_first)
    return sub_layer(
        carried, gain_second, up_second, up_scale_second, down_second, down_scale_second
    )


def solution(mesh):
    in_specs = (
        P("dp", "ra"),
        P("ra"),
        P("ra", "cb"),
        P("cb"),
        P("cb", "ra"),
        P("ra"),
        P("ra"),
        P("ra", "cb"),
        P("cb"),
        P("cb", "ra"),
        P("ra"),
    )
    out_specs = P("dp", "ra")
    return jax.shard_map(shards, mesh=mesh, in_specs=in_specs, out_specs=out_specs, check_vma=False)
```

profile of v0, /device:TPU:0, one launch (start us, length us, event | category | flops | bytes accessed | tf_op | source)
XLA Modules:
  0.0 241.5 jit_solution(8065290762153675405)
XLA Ops:
  6.5 0.0 reduce-scatter.3.cloned.1.call-start
  6.5 0.7 convert_element_type.59
  7.2 1.0 fusion.16
  8.3 13.5 %psum.28 = f32[64,1]{0,1:T(1,128)S(1)} all-reduce(f32[64,1]{0,1:T(1,128)S(1)} %bitcast.9), channel_id=1, replica_groups=mesh['ra'=4,'cb'=4,'dp'=2] {'ra'}, use_global_device_ids=true, to_apply=%region_1.0 | all-reduce | flops 64 | bytes 512 | tf_op jit(solution)/shard_map/psum | solution.py:13
  21.8 0.0 copy-start.3
  21.8 0.0 copy-start
  21.8 0.0 copy-start.1
  21.8 8.5 %fusion.6 = f32[64,4096]{1,0:T(8,128)} fusion(f32[1024,4096]{1,0:T(8,128)} %param.13, bf16[64,1024]{1,0:T(8,128)(2,1)} %param.11, f32[1024]{0:T(1024)S(1)} %convert_element_type.59, f32[64]{0:T(128)S(1)} %rsqrt_bitcast_fusion.1), kind=kOutput, calls=%fused_computation.6 | convolution fusion | flops 541327360 | bytes 17961216 | tf_op jit(solution)/shard_map/dot_general | solution.py:16
  30.3 0.0 reduce-scatter.3.cloned.1.call-update
  30.3 0.0 all-reduce.3.cloned.1.call-start
  30.4 0.7 dynamic_slice.6
  31.1 24.9 %reduce-scatter.3.cloned.1.call-done = f32[64,1024]{1,0:T(8,128)} async-done(((f32[64,4096]{1,0:T(8,128)}), f32[64,1024]{1,0:T(8,128)}) %reduce-scatter.3.cloned.1.call-update) | async-done | bytes 262160 | tf_op jit(solution)/shard_map/reduce_scatter | solution.py:19
  56.0 1.0 multiply_convert_fusion.1
  56.9 16.0 %all_gather.6 = bf16[64,4096]{1,0:T(8,128)(2,1)S(1)} all-gather(bf16[64,1024]{1,0:T(8,128)(2,1)S(1)} %multiply_convert_fusion.1), channel_id=1, replica_groups=mesh['ra'=4,'cb'=4,'dp'=2] {'ra'}, dimensions={1}, use_global_device_ids=true | all-gather | bytes 655360 | tf_op jit(solution)/shard_map/all_gather | solution.py:25
  73.0 0.0 dynamic-slice-start
  73.0 8.0 %fusion.8 = bf16[64,1024]{1,0:T(8,128)(2,1)} fusion(bf16[64,4096]{1,0:T(8,128)(2,1)S(1)} %all_gather.6, f32[4096,1024]{1,0:T(8,128)} %param.15), kind=kOutput, calls=%fused_computation.8 | convolution fusion | flops 541130752 | bytes 17432576 | tf_op jit(solution)/shard_map/dot_general | solution.py:26
  81.0 0.0 all-reduce.3.cloned.1.call-update
  81.0 0.0 reduce-scatter.5.cloned.1.call-start
  81.1 0.0 copy-done.3
  81.1 40.6 %all-reduce.3.cloned.1.call-done = bf16[64,1024]{1,0:T(8,128)(2,1)} async-done(((bf16[64,1024]{1,0:T(8,128)(2,1)}), bf16[64,1024]{1,0:T(8,128)(2,1)}) %all-reduce.3.cloned.1.call-update) | async-done | bytes 131088 | tf_op jit(solution)/shard_map/psum | solution.py:30
  121.7 0.0 copy-done
  121.7 0.0 copy-done.1
  121.7 1.1 fusion.21
  122.8 11.7 %psum.30 = f32[64,1]{0,1:T(1,128)S(1)} all-reduce(f32[64,1]{0,1:T(1,128)S(1)} %bitcast.8), channel_id=1, replica_groups=mesh['ra'=4,'cb'=4,'dp'=2] {'ra'}, use_global_device_ids=true, to_apply=%region_5.6 | all-reduce | flops 64 | bytes 512 | tf_op jit(solution)/shard_map/psum | solution.py:13
  134.5 0.0 copy-start.2
  134.5 8.4 %fusion.2 = f32[64,4096]{1,0:T(8,128)} fusion(f32[1024,4096]{1,0:T(8,128)} %param.18, bf16[64,1024]{1,0:T(8,128)(2,1)S(1)} %get-tuple-element.6, f32[1024]{0:T(1024)S(1)} %convert_element_type.68, f32[64]{0:T(128)S(1)} %rsqrt_bitcast_fusion), kind=kOutput, calls=%fused_computation.2 | convolution fusion | flops 541327360 | bytes 17961216 | tf_op jit(solution)/shard_map/dot_general | solution.py:16
  142.9 0.0 reduce-scatter.5.cloned.1.call-update
  143.0 0.0 all-reduce.5.cloned.1.call-start
  143.0 24.6 %reduce-scatter.5.cloned.1.call-done = f32[64,1024]{1,0:T(8,128)} async-done(((f32[64,4096]{1,0:T(8,128)}), f32[64,1024]{1,0:T(8,128)}) %reduce-scatter.5.cloned.1.call-update) | async-done | bytes 262160 | tf_op jit(solution)/shard_map/reduce_scatter | solution.py:19
  167.6 0.0 dynamic-slice-done
  167.6 1.0 multiply_convert_fusion
  168.6 15.9 %all_gather.7 = bf16[64,4096]{1,0:T(8,128)(2,1)S(1)} all-gather(bf16[64,1024]{1,0:T(8,128)(2,1)S(1)} %multiply_convert_fusion), channel_id=1, replica_groups=mesh['ra'=4,'cb'=4,'dp'=2] {'ra'}, dimensions={1}, use_global_device_ids=true | all-gather | bytes 655360 | tf_op jit(solution)/shard_map/all_gather | solution.py:25
  184.5 8.0 %fusion.11 = bf16[64,1024]{1,0:T(8,128)(2,1)} fusion(bf16[64,4096]{1,0:T(8,128)(2,1)S(1)} %all_gather.7, f32[4096,1024]{1,0:T(8,128)} %param.20), kind=kOutput, calls=%fused_computation.9 | convolution fusion | flops 541130752 | bytes 17432576 | tf_op jit(solution)/shard_map/dot_general | solution.py:26
  192.6 0.0 all-reduce.5.cloned.1.call-update
  192.6 40.8 %all-reduce.5.cloned.1.call-done = bf16[64,1024]{1,0:T(8,128)(2,1)} async-done(((bf16[64,1024]{1,0:T(8,128)(2,1)}), bf16[64,1024]{1,0:T(8,128)(2,1)}) %all-reduce.5.cloned.1.call-update) | async-done | bytes 131088 | tf_op jit(solution)/shard_map/psum | solution.py:30
  233.4 0.0 copy-done.2
  233.4 1.6 fusion.20
  (3 shorter events, 0.0 us)
Async XLA Ops:
  6.5 49.4 %reduce-scatter.3.cloned.1.call-start = ((), (), s32[]{:S(2)}) async-start(), calls=%async_computation.2 | async-start | bytes 1310720 | tf_op jit(solution)/shard_map/reduce_scatter | solution.py:19
  21.8 59.3 %copy-start.3 = (bf16[1024]{0:T(1024)(128)(2,1)S(1)}, bf16[1024]{0:T(1024)(128)(2,1)}, u32[]{:S(2)}) copy-start(bf16[1024]{0:T(1024)(128)(2,1)} %param.17) | copy-start | bytes 6148
  21.8 100.0 %copy-start = (bf16[64,1024]{1,0:T(8,128)(2,1)S(1)}, bf16[64,1024]{1,0:T(8,128)(2,1)}, u32[]{:S(2)}) copy-start(bf16[64,1024]{1,0:T(8,128)(2,1)} %param.11) | copy-start | bytes 393220
  21.8 100.0 %copy-start.1 = (f32[1024]{0:T(1024)S(1)}, f32[1024]{0:T(1024)}, u32[]{:S(2)}) copy-start(f32[1024]{0:T(1024)} %param.16) | copy-start | bytes 12292
  30.3 91.4 %all-reduce.3.cloned.1.call-start = ((), (), s32[]{:S(2)}) async-start(), calls=%async_computation.3 | async-start | bytes 262144 | tf_op jit(solution)/shard_map/psum | solution.py:30
  73.0 94.7 %dynamic-slice-start = ((f32[4096]{0:T(1024)}, s32[]{:T(128)}), f32[1024]{0:T(1024)S(1)}, s32[]{:S(2)}) async-start(f32[4096]{0:T(1024)} %param.19, s32[]{:T(128)} %select_n.4), calls=%async_computation.6 | async-start | bytes 8704 | tf_op jit(solution)/shard_map/dynamic_slice | solution.py:21
  81.0 86.6 %reduce-scatter.5.cloned.1.call-start = ((), (), s32[]{:S(2)}) async-start(), calls=%async_computation.4 | async-start | bytes 1310720 | tf_op jit(solution)/shard_map/reduce_scatter | solution.py:19
  134.5 98.8 %copy-start.2 = (f32[1024]{0:T(1024)S(1)}, f32[1024]{0:T(1024)}, u32[]{:S(2)}) copy-start(f32[1024]{0:T(1024)} %param.21) | copy-start | bytes 12292
  143.0 90.4 %all-reduce.5.cloned.1.call-start = ((), (), s32[]{:S(2)}) async-start(), calls=%async_computation.5 | async-start | bytes 262144 | tf_op jit(solution)/shard_map/psum | solution.py:30
Sparse Core Ops, SparseCore 0:
  30.4 25.4 reduce-scatter.2
  81.1 40.5 all-reduce.2
  143.1 24.5 reduce-scatter.4
  192.7 40.5 all-reduce.4
where the time goes:
time: 242 us
  waiting for transfers between devices  131 us (54%)
  blocking collectives  57.1 us (24%)
  matrix products  33 us (14%)
  between operations  13.2 us (5%)
  other arithmetic  6.38 us (3%)
    psum x2, waiting for transfers between devices, sub_layer(): total = lax.psum(projected.astype(jnp.bfloat16), 'cb').astype(jnp.float32)  81.4 us
    reduce_scatter x2, waiting for transfers between devices, sub_layer(): lax.psum_scatter(partial_value, 'ra', scatter_dimension=1, tiled=True)  49.5 us
    all_gather x2, blocking collectives, sub_layer(): hidden = lax.all_gather(own_units, 'ra', axis=1, tiled=True)  31.9 us
    psum x2, blocking collectives, sub_layer(): squares = lax.psum(jnp.sum(values * values, axis=1, keepdims=True), 'ra')  25.2 us
    dot_general x2, matrix products, sub_layer(): jnp.dot(normed, up_weight.astype(jnp.bfloat16), preferred_element_type=jn...  16.9 us
    dot_general x2, matrix products, sub_layer(): jnp.dot(hidden, down_weight.astype(jnp.bfloat16), preferred_element_type=...  16.1 us
  transfers between devices with their start and end apart: 4, of which 4 were waited for; matrix products, arithmetic and copies ran while one was open for 0% of the time, Pallas kernels for 0%

commit v1 on v0

--- a/solution.py
+++ b/solution.py
@@ -27,7 +27,9 @@
         hidden, down_weight.astype(jnp.bfloat16), preferred_element_type=jnp.float32
     ).astype(jnp.bfloat16)
     projected = lax.optimization_barrier(projected).astype(jnp.float32)
-    total = lax.psum(projected.astype(jnp.bfloat16), "cb").astype(jnp.float32)
+    total = jnp.sum(lax.all_gather(projected.astype(jnp.bfloat16), "cb"), axis=0).astype(
+        jnp.float32
+    )
     return (residual_share * values + total * down_scale).astype(jnp.bfloat16)
 
 

time: 242 us -> 176 us (0.73)
  waiting for transfers between devices: 131 us -> 50.9 us
  blocking collectives: 57.1 us -> 74 us
    psum x2 -> x0, waiting for transfers between devices: 81.4 us -> none  [sub_layer(): total = lax.psum(projected.astype(jnp.bfloat16), 'cb').astype(jnp.float32)]
    all_gather x0 -> x2, blocking collectives: none -> 20 us  [sub_layer(): lax.all_gather(projected.astype(jnp.bfloat16), 'cb')]
    psum x2, blocking collectives: 25.2 us -> 22 us  [sub_layer(): squares = lax.psum(jnp.sum(values * values, axis=1, keepdims=True), 'ra')]
  transfers between devices with their start and end apart: 4 -> 2, of which waited for: 4 -> 2; matrix products, arithmetic and copies ran while one was open for 0% -> 0% of each run, Pallas kernels for 0% -> 0%
where the time goes in v1:
time: 176 us
  blocking collectives  74 us (42%)
  waiting for transfers between devices  50.9 us (29%)
  matrix products  31.7 us (18%)
  between operations  13.5 us (8%)
  other arithmetic  4.75 us (3%)
    reduce_scatter x2, waiting for transfers between devices, sub_layer(): lax.psum_scatter(partial_value, 'ra', scatter_dimension=1, tiled=True)  50.9 us
    all_gather x2, blocking collectives, sub_layer(): hidden = lax.all_gather(own_units, 'ra', axis=1, tiled=True)  32 us
    psum x2, blocking collectives, sub_layer(): squares = lax.psum(jnp.sum(values * values, axis=1, keepdims=True), 'ra')  22 us
    all_gather x2, blocking collectives, sub_layer(): lax.all_gather(projected.astype(jnp.bfloat16), 'cb')  20 us
    dot_general x2, matrix products, sub_layer(): jnp.dot(normed, up_weight.astype(jnp.bfloat16), preferred_element_type=jn...  16.9 us
    dot_general x2, matrix products, sub_layer(): jnp.dot(hidden, down_weight.astype(jnp.bfloat16), preferred_element_type=...  14.8 us
  transfers between devices with their start and end apart: 2, of which 2 were waited for; matrix products, arithmetic and copies ran while one was open for 0% of the time, Pallas kernels for 0%

profile of v1, /device:TPU:0, one launch (start us, length us, event | category | flops | bytes accessed | tf_op | source)
XLA Modules:
  0.0 175.6 jit_solution(9456167654614371704)
XLA Ops:
  6.5 0.0 copy-start.3
  6.5 0.0 reduce-scatter.3.cloned.1.call-start
  6.5 0.7 convert_element_type.63
  7.2 1.0 fusion.16
  8.3 13.5 %psum.14 = f32[64,1]{0,1:T(1,128)S(1)} all-reduce(f32[64,1]{0,1:T(1,128)S(1)} %bitcast.13), channel_id=1, replica_groups=mesh['ra'=4,'cb'=4,'dp'=2] {'ra'}, use_global_device_ids=true, to_apply=%region_1.0 | all-reduce | flops 64 | bytes 512 | tf_op jit(solution)/shard_map/psum | solution.py:13
  21.8 0.0 copy-start
  21.8 0.0 copy-start.1
  21.8 8.5 %fusion.6 = f32[64,4096]{1,0:T(8,128)} fusion(f32[1024,4096]{1,0:T(8,128)} %param.13, bf16[64,1024]{1,0:T(8,128)(2,1)} %param.11, f32[1024]{0:T(1024)S(1)} %convert_element_type.63, f32[64]{0:T(128)S(1)} %rsqrt_bitcast_fusion.1), kind=kOutput, calls=%fused_computation.6 | convolution fusion | flops 541327360 | bytes 17961216 | tf_op jit(solution)/shard_map/dot_general | solution.py:16
  30.3 0.0 reduce-scatter.3.cloned.1.call-update
  30.3 0.0 reduce-scatter.5.cloned.1.call-start
  30.4 0.0 copy-done.3
  30.4 0.7 dynamic_slice.6
  31.1 24.9 %reduce-scatter.3.cloned.1.call-done = f32[64,1024]{1,0:T(8,128)} async-done(((f32[64,4096]{1,0:T(8,128)}), f32[64,1024]{1,0:T(8,128)}) %reduce-scatter.3.cloned.1.call-update) | async-done | bytes 262160 | tf_op jit(solution)/shard_map/reduce_scatter | solution.py:19
  56.0 1.0 multiply_convert_fusion.1
  56.9 16.0 %all_gather.18 = bf16[64,4096]{1,0:T(8,128)(2,1)S(1)} all-gather(bf16[64,1024]{1,0:T(8,128)(2,1)S(1)} %multiply_convert_fusion.1), channel_id=1, replica_groups=mesh['ra'=4,'cb'=4,'dp'=2] {'ra'}, dimensions={1}, use_global_device_ids=true | all-gather | bytes 655360 | tf_op jit(solution)/shard_map/all_gather | solution.py:25
  72.9 0.0 dynamic-slice-start
  72.9 7.4 %fusion.8 = bf16[64,1024]{1,0:T(8,128)(2,1)S(1)} fusion(bf16[64,4096]{1,0:T(8,128)(2,1)S(1)} %all_gather.18, f32[4096,1024]{1,0:T(8,128)} %param.15), kind=kOutput, calls=%fused_computation.8 | convolution fusion | flops 541130752 | bytes 17432576 | tf_op jit(solution)/shard_map/dot_general | solution.py:26
  80.3 10.0 %all-gather = bf16[256,1024]{1,0:T(8,128)(2,1)S(1)} all-gather(bf16[64,1024]{1,0:T(8,128)(2,1)S(1)} %fusion.8), channel_id=2, replica_groups=mesh['ra'=4,'cb'=4,'dp'=2] {'cb'}, dimensions={0}, use_global_device_ids=true | all-gather | bytes 655360 | tf_op jit(solution)/shard_map/all_gather | solution.py:30
  90.3 0.1 reduce_sum.43
  90.4 0.0 copy-done
  90.4 0.0 copy-done.1
  90.4 0.2 fusion.21
  90.6 8.5 %psum.15 = f32[64,1]{0,1:T(1,128)S(1)} all-reduce(f32[64,1]{0,1:T(1,128)S(1)} %bitcast.12), channel_id=1, replica_groups=mesh['ra'=4,'cb'=4,'dp'=2] {'ra'}, use_global_device_ids=true, to_apply=%region_5.6 | all-reduce | flops 64 | bytes 512 | tf_op jit(solution)/shard_map/psum | solution.py:13
  99.1 0.0 copy-start.2
  99.1 8.4 %fusion.2 = f32[64,4096]{1,0:T(8,128)} fusion(f32[1024,4096]{1,0:T(8,128)} %param.18, bf16[64,1024]{1,0:T(8,128)(2,1)S(1)} %get-tuple-element.6, f32[1024]{0:T(1024)S(1)} %convert_element_type.72, f32[64]{0:T(128)S(1)} %rsqrt_bitcast_fusion), kind=kOutput, calls=%fused_computation.2 | convolution fusion | flops 541327360 | bytes 17961216 | tf_op jit(solution)/shard_map/dot_general | solution.py:16
  107.6 0.0 reduce-scatter.5.cloned.1.call-update
  107.6 26.0 %reduce-scatter.5.cloned.1.call-done = f32[64,1024]{1,0:T(8,128)} async-done(((f32[64,4096]{1,0:T(8,128)}), f32[64,1024]{1,0:T(8,128)}) %reduce-scatter.5.cloned.1.call-update) | async-done | bytes 262160 | tf_op jit(solution)/shard_map/reduce_scatter | solution.py:19
  133.6 0.0 dynamic-slice-done
  133.6 1.0 multiply_convert_fusion
  134.6 16.0 %all_gather.21 = bf16[64,4096]{1,0:T(8,128)(2,1)S(1)} all-gather(bf16[64,1024]{1,0:T(8,128)(2,1)S(1)} %multiply_convert_fusion), channel_id=1, replica_groups=mesh['ra'=4,'cb'=4,'dp'=2] {'ra'}, dimensions={1}, use_global_device_ids=true | all-gather | bytes 655360 | tf_op jit(solution)/shard_map/all_gather | solution.py:25
  150.6 7.4 %fusion.11 = bf16[64,1024]{1,0:T(8,128)(2,1)S(1)} fusion(bf16[64,4096]{1,0:T(8,128)(2,1)S(1)} %all_gather.21, f32[4096,1024]{1,0:T(8,128)} %param.20), kind=kOutput, calls=%fused_computation.9 | convolution fusion | flops 541130752 | bytes 17432576 | tf_op jit(solution)/shard_map/dot_general | solution.py:26
  158.0 10.0 %all-gather.1 = bf16[256,1024]{1,0:T(8,128)(2,1)S(1)} all-gather(bf16[64,1024]{1,0:T(8,128)(2,1)S(1)} %fusion.11), channel_id=3, replica_groups=mesh['ra'=4,'cb'=4,'dp'=2] {'cb'}, dimensions={0}, use_global_device_ids=true | all-gather | bytes 655360 | tf_op jit(solution)/shard_map/all_gather | solution.py:30
  168.0 0.1 reduce_sum.45
  168.1 0.0 copy-done.2
  168.1 0.7 fusion.20
  (3 shorter events, 0.0 us)
Async XLA Ops:
  6.5 23.8 %copy-start.3 = (bf16[1024]{0:T(1024)(128)(2,1)S(1)}, bf16[1024]{0:T(1024)(128)(2,1)}, u32[]{:S(2)}) copy-start(bf16[1024]{0:T(1024)(128)(2,1)} %param.17) | copy-start | bytes 6148
  6.5 49.4 %reduce-scatter.3.cloned.1.call-start = ((), (), s32[]{:S(2)}) async-start(), calls=%async_computation.2 | async-start | bytes 1310720 | tf_op jit(solution)/shard_map/reduce_scatter | solution.py:19
  21.8 68.6 %copy-start = (bf16[64,1024]{1,0:T(8,128)(2,1)S(1)}, bf16[64,1024]{1,0:T(8,128)(2,1)}, u32[]{:S(2)}) copy-start(bf16[64,1024]{1,0:T(8,128)(2,1)} %param.11) | copy-start | bytes 393220
  21.8 68.7 %copy-start.1 = (f32[1024]{0:T(1024)S(1)}, f32[1024]{0:T(1024)}, u32[]{:S(2)}) copy-start(f32[1024]{0:T(1024)} %param.16) | copy-start | bytes 12292
  30.3 103.3 %reduce-scatter.5.cloned.1.call-start = ((), (), s32[]{:S(2)}) async-start(), calls=%async_computation.3 | async-start | bytes 1310720 | tf_op jit(solution)/shard_map/reduce_scatter | solution.py:19
  72.9 60.7 %dynamic-slice-start = ((f32[4096]{0:T(1024)}, s32[]{:T(128)}), f32[1024]{0:T(1024)S(1)}, s32[]{:S(2)}) async-start(f32[4096]{0:T(1024)} %param.19, s32[]{:T(128)} %select_n.4), calls=%async_computation.4 | async-start | bytes 8704 | tf_op jit(solution)/shard_map/dynamic_slice | solution.py:21
  99.1 68.9 %copy-start.2 = (f32[1024]{0:T(1024)S(1)}, f32[1024]{0:T(1024)}, u32[]{:S(2)}) copy-start(f32[1024]{0:T(1024)} %param.21) | copy-start | bytes 12292
Sparse Core Ops, SparseCore 0:
  30.4 25.4 reduce-scatter.2
  107.7 25.8 reduce-scatter.4
